TPU v7x, 512 devices: a whole 4x8x8 slice. The times are simulated.
512 devices in a mesh: sp: 64 (over z, y), fs: 4 (over x), tp: 2 (over core).
Axes of the slice: x: 4, y: 8, z: 8, core: 2. Of those that a mesh axis runs over, the one named last changes fastest.
Arguments:
- tokens: bfloat16 [4, 8192, 2048], P('fs', ('sp', 'tp')), may hold values from -6 to 6
- input_norm_gain: float32 [2048], replicated, may hold values from 0.1 to 1.9
- pooling_input_weight: bfloat16 [2048, 1024], P('sp', 'tp'), may hold values from -0.125 to 0.125
- query_weight: bfloat16 [2048, 1024], P('sp', 'tp'), may hold values from -0.125 to 0.125
- forget_weight: bfloat16 [2048, 1024], P('sp', 'tp'), may hold values from -0.125 to 0.125
- value_weight: bfloat16 [2048, 1024], P('sp', 'tp'), may hold values from -0.125 to 0.125
- pooling_group_maps: bfloat16 [4, 256, 256], P('tp'), may hold values from -0.375 to 0.375
- pooling_scale: float32 [1024], P('tp'), may hold values from 0.1 to 1.9
- lower_bound_logits: float32 [1024], P('tp')
- decay_spike: float32 [4, 8192, 8], P('fs', 'sp', 'tp'), may hold values from -0.75 to 0
- head_norm_gain: float32 [1024], P('tp'), may hold values from 0.1 to 1.9
- pooling_output_weight: bfloat16 [1024, 2048], P('tp', 'sp'), may hold values from -0.125 to 0.125
- recurrent_output_weight: bfloat16 [1024, 2048], P('tp', 'sp'), may hold values from -0.125 to 0.125
Outputs:
- mixed: bfloat16 [4, 8192, 2048], P('fs', ('sp', 'tp'))
All inputs are finite; a program needn't handle non-finite values.
Results may differ from a plain program's by a relative error of at most 0.013.
Values may be sent and summed in bfloat16 or wider, within the bound.
A program may use at most 64 MiB of HBM per device.

v0:
```python
import jax
import jax.numpy as jnp
from jax import lax
from jax.sharding import Mesh
from jax.sharding import PartitionSpec as P

BLOCK = 64
SP = ("sp_0", "sp_1")
SP_TP = ("sp_0", "sp_1", "tp")
EPSILON = 1e-06
HIGHEST = lax.Precision.HIGHEST


def in_order(tiles, dim):
    tiles = jnp.moveaxis(tiles, 0, dim)
    dims = tiles.shape
    return tiles.reshape(*dims[:dim], dims[dim] * dims[dim + 1], *dims[dim + 2 :])


def all_blocks(shard, axes, sequence):
    tiles = shard
    for k in sequence:
        tiles = lax.all_gather(tiles, axes[k])
    done = sequence[::-1]
    back = [done.index(k) for k in range(len(axes))]
    tiles = tiles.transpose(*back, *range(len(axes), tiles.ndim))
    return tiles.reshape(-1, *shard.shape)


def gathered_by_axis(shard, axes, sequence, dim):
    return in_order(all_blocks(shard, axes, sequence), dim)


def shifted(value, axis, steps):
    count = lax.axis_size(axis)
    first, last = (max(0, -steps), min(count, count - steps))
    return lax.ppermute(value, axis, [(source, source + steps) for source in range(first, last)])


def filled_with(shard, identity):
    return jax.tree.map(
        lambda part, zero: jnp.zeros_like(part) + jnp.asarray(zero, part.dtype), shard, identity
    )


def carried_in(shard, axes, combine, identity):
    before = start = filled_with(shard, identity)
    total = shard
    for axis in reversed(axes):
        peers, here = (lax.axis_size(axis), lax.axis_index(axis))
        pieces = jax.tree.map(
            lambda part, kind: lax.all_gather(part.astype(kind), axis),
            total,
            (jnp.bfloat16, jnp.bfloat16),
        )
        inside, total = (start, start)
        for k in range(peers):
            passed = k < here
            total = combine(
                total, jax.tree.map(lambda part, own: part[k].astype(own.dtype), pieces, shard)
            )
            inside = jax.tree.map(lambda new, old: jnp.where(passed, new, old), total, inside)
        before = combine(inside, before)
    return before


def cut_along(shard, dim, peers):
    before, after = (shard.shape[:dim], shard.shape[dim + 1 :])
    return jnp.moveaxis(shard.reshape(*before, peers, -1, *after), dim, 0)


def summed_on_arrival(shard, axis, dim):
    tiles = cut_along(shard, dim, lax.axis_size(axis))
    arrived = lax.all_to_all(tiles, axis, split_axis=0, concat_axis=0, tiled=True)
    return arrived.astype(jnp.float32).sum(axis=0)


def rms_scale(values, gain):
    return values * lax.rsqrt(jnp.mean(values * values, axis=-1, keepdims=True) + EPSILON) * gain


def join_state(earlier, later):
    decay_one, state_one = earlier
    decay_two, state_two = later
    return (decay_one * decay_two, decay_two[..., None] * state_one + state_two)


def body(
    tokens,
    input_norm_gain,
    pooling_input_weight,
    query_weight,
    forget_weight,
    value_weight,
    pooling_group_maps,
    pooling_scale,
    lower_bound_logits,
    decay_spike,
    head_norm_gain,
    pooling_output_weight,
    recurrent_output_weight,
):
    gathered = lax.all_gather(tokens, "tp", axis=1, tiled=True)[0]
    length_total = gathered.shape[0]
    normed = rms_scale(gathered.astype(jnp.float32), input_norm_gain).astype(jnp.bfloat16)
    pool_width = pooling_input_weight.shape[1]
    rec_width = query_weight.shape[1]
    stacked = jnp.concatenate(
        [pooling_input_weight, query_weight, forget_weight, value_weight], axis=1
    )
    out_local = jnp.concatenate([pooling_output_weight, recurrent_output_weight], axis=0)
    projected = jnp.dot(
        normed, lax.all_gather(stacked, SP, axis=0, tiled=True), preferred_element_type=jnp.float32
    )
    out_full = gathered_by_axis(out_local, SP, (0, 1), 1)
    rounded = lax.optimization_barrier(projected.astype(jnp.bfloat16))
    pool_input = rounded[:, :pool_width]
    query_matrix = rounded[:, pool_width : pool_width + rec_width].astype(jnp.float32)
    forget_gate_logit = rounded[:, pool_width + rec_width : pool_width + 2 * rec_width].astype(
        jnp.float32
    )
    value_projected = rounded[:, pool_width + 2 * rec_width :].astype(jnp.float32)
    groups_local = pooling_group_maps.shape[0]
    group_size = pooling_group_maps.shape[1]
    reach_rows = 2 ** (groups_local * lax.axis_size("tp"))
    previous = shifted(pool_input[length_total - reach_rows :], SP, 1)
    extended = jnp.concatenate([previous, pool_input], axis=0).astype(jnp.float32)
    extended = extended.reshape(reach_rows + length_total, groups_local, group_size)
    group_ids = lax.axis_index("tp") * groups_local + jnp.arange(groups_local, dtype=jnp.int32)
    windows = jnp.left_shift(jnp.int32(2), group_ids)
    window_sum = jnp.zeros((length_total, groups_local, group_size), jnp.float32)
    for offset in range(reach_rows):
        inside = (offset < windows).astype(jnp.float32)
        window_sum = (
            window_sum
            + extended[reach_rows - offset : reach_rows - offset + length_total] * inside[:, None]
        )
    position_index = lax.axis_index(SP) * length_total + jnp.arange(length_total, dtype=jnp.int32)
    counts = jnp.minimum(position_index[:, None] + 1, windows[None, :]).astype(jnp.float32)
    pool_diff = (window_sum / counts[:, :, None] - extended[reach_rows:]).astype(jnp.bfloat16)
    pool_mapped = jnp.einsum(
        "tgc,gcd->tgd", pool_diff, pooling_group_maps, preferred_element_type=jnp.float32
    )
    pool_out = (pool_mapped.reshape(length_total, pool_width) * pooling_scale).astype(jnp.bfloat16)
    local_heads = decay_spike.shape[2]
    head_width = rec_width // local_heads
    blocks = length_total // BLOCK
    block_layout = (blocks, BLOCK, local_heads, head_width)
    reader = jax.nn.silu(query_matrix).reshape(block_layout)
    key_gate_value = jax.nn.sigmoid(-lower_bound_logits) * jax.nn.sigmoid(-forget_gate_logit)
    decay_logarithm = (
        jnp.log1p(-key_gate_value).reshape(length_total, local_heads, head_width)
        + decay_spike[0][:, :, None]
    ).reshape(block_layout)
    key_rows = key_gate_value.reshape(block_layout)
    value_rows = value_projected.reshape(block_layout)
    inner_log = jnp.cumsum(decay_logarithm, axis=1)
    read_scaled = reader * jnp.exp(inner_log)
    key_scaled = key_rows * jnp.exp(-inner_log)
    causal = (jnp.arange(BLOCK)[:, None] >= jnp.arange(BLOCK)[None, :]).astype(jnp.float32)
    scores = jnp.einsum("nthd,nshd->nhts", read_scaled, key_scaled, precision=HIGHEST) * causal
    within = jnp.einsum("nhts,nshe->nthe", scores, value_rows, precision=HIGHEST)
    closing = inner_log[:, -1]
    key_tail = key_rows * jnp.exp(closing[:, None] - inner_log)
    deltas = jnp.einsum("nshd,nshe->nhde", key_tail, value_rows, precision=HIGHEST)
    block_decay = jnp.exp(closing)

    def advance(carried, input_batch):
        decay_now, delta_now = input_batch
        return (decay_now[..., None] * carried + delta_now, carried)

    initial = jnp.zeros((local_heads, head_width, head_width), jnp.float32)
    device_state, entry_states = lax.scan(advance, initial, (block_decay, deltas))
    device_decay = jnp.exp(jnp.sum(closing, axis=0))
    scanned = carried_in(
        (device_decay, device_state),
        SP,
        join_state,
        (jnp.ones_like(device_decay), jnp.zeros_like(device_state)),
    )
    prior_state = scanned[1]
    before = jnp.cumsum(closing, axis=0) - closing
    start_states = entry_states + jnp.exp(before)[..., None] * prior_state[None]
    read_out = within + jnp.einsum("nthd,nhde->nthe", read_scaled, start_states, precision=HIGHEST)
    read_out = read_out.reshape(length_total, local_heads, head_width)
    recurrent_output = (
        rms_scale(read_out, 1.0).reshape(length_total, rec_width) * head_norm_gain
    ).astype(jnp.bfloat16)
    mixed_rows = jnp.concatenate([pool_out, recurrent_output], axis=1)
    summed = summed_on_arrival(
        jnp.dot(mixed_rows, out_full, preferred_element_type=jnp.float32).astype(jnp.bfloat16),
        "tp",
        0,
    )
    return summed.astype(jnp.bfloat16)[None]


def solution(mesh):
    torus = Mesh(
        mesh.devices.reshape(8, 8, mesh.shape["fs"], mesh.shape["tp"]), ("sp_0", "sp_1", "fs", "tp")
    )
    return jax.shard_map(
        body,
        mesh=torus,
        in_specs=(
            P("fs", SP_TP, None),
            P(),
            P(SP, "tp"),
            P(SP, "tp"),
            P(SP, "tp"),
            P(SP, "tp"),
            P("tp", None, None),
            P("tp"),
            P("tp"),
            P("fs", SP, "tp"),
            P("tp"),
            P("tp", SP),
            P("tp", SP),
        ),
        out_specs=P("fs", SP_TP, None),
        check_vma=False,
    )
```

profile of v0, /device:TPU:1, one launch (start us, length us, event | category | flops | bytes accessed | tf_op | source)
XLA Modules:
  0.0 277.8 jit_solution(2328554561795465922)
XLA Ops:
  6.5 1.5 pad_maximum_fusion
  8.1 0.0 all-gather.16.cloned.1.call-start
  8.1 0.8 pad_maximum_fusion.1
  8.9 27.3 %all-gather.2 = bf16[8192,32]{0,1:T(8,128)(2,1)S(1)} all-gather(bf16[1024,32]{0,1:T(8,128)(2,1)S(1)} %pad_maximum_fusion.1), channel_id=4, replica_groups=mesh['sp_0'=8,'sp_1'=8,'fs'=4,'tp'=2] {'sp_0'}, dimensions={0}, use_global_device_ids=true | all-gather | bytes 589824 | tf_op jit(solution)/shard_map/all_gather | solution.py:23
  36.2 1.1 copy.197
  37.4 0.0 all-gather.14.cloned.1.call-start
  37.5 0.8 copy.177
  38.3 7.8 %all_gather.36 = bf16[1,128,2048]{2,1,0:T(8,128)(2,1)S(1)} all-gather(bf16[1,64,2048]{2,1,0:T(8,128)(2,1)} %param.15), channel_id=1, replica_groups=mesh['sp_0'=8,'sp_1'=8,'fs'=4,'tp'=2] {'tp'}, dimensions={1}, use_global_device_ids=true | all-gather | bytes 786432 | tf_op jit(solution)/shard_map/all_gather | solution.py:103
  46.2 0.2 fusion.2
  46.4 0.7 add_divide_fusion
  47.0 67.8 %all-gather.10.cloned.1.call-done = bf16[2048,2048]{1,0:T(8,128)(2,1)} async-done(((bf16[32,2048]{1,0:T(8,128)(2,1)}), bf16[2048,2048]{1,0:T(8,128)(2,1)}) %all-gather.10.cloned.1.call-update) | async-done | bytes 8388624 | tf_op jit(solution)/shard_map/all_gather | solution.py:113
  114.9 4.7 %convolution_convert_fusion = bf16[128,2048]{1,0:T(8,128)(2,1)S(1)} fusion(bf16[2048,2048]{1,0:T(8,128)(2,1)} %all-gather.10.cloned.1.call-done, bf16[1,128,2048]{2,1,0:T(8,128)(2,1)S(1)} %all_gather.36, f32[2048]{0:T(1024)} %param.16, f32[128]{0:T(128)S(1)} %add_rsqrt_fusion.1), kind=kOutput, calls=%fused_computation.3 | convolution fusion | flops 1075052544 | bytes 9445888 | tf_op jit(solution)/shard_map/dot_general | solution.py:112
  119.6 0.2 negate_log-plus-one_fusion
  119.8 0.1 reshape.384
  119.9 0.1 reshape.383
  120.0 0.1 reshape.385
  120.2 0.2 fusion.54
  120.4 0.2 exponential_multiply_fusion
  120.6 0.6 fusion.48
  121.2 0.5 while.13
  121.3 0.2 bitcast_add_fusion.2
  121.5 0.2 bitcast_add_fusion.2
  121.7 0.7 convert_element_type.533
  122.4 0.0 all-gather.12.cloned.1.call-start
  122.6 0.1 minimum_convert_fusion
  122.7 49.5 %all-gather.16.cloned.1.call-done = bf16[64,1024,32]{1,0,2:T(8,128)(2,1)} async-done(((bf16[8,1024,32]{1,0,2:T(8,128)(2,1)}), bf16[64,1024,32]{1,0,2:T(8,128)(2,1)}) %all-gather.16.cloned.1.call-update) | async-done | bytes 4194320 | tf_op jit(solution)/shard_map/all_gather | solution.py:23
  172.2 6.5 %copy.176 = bf16[8,8,1024,32]{2,3,1,0:T(8,128)(2,1)} copy(bf16[8,8,1024,32]{2,0,1,3:T(8,128)(2,1)} %bitcast.379) | data formatting | bytes 8388608 | tf_op jit(solution)/shard_map/transpose | solution.py:26
  178.7 11.0 %all-gather.4 = bf16[8,4,128]{2,1,0:T(4,128)(2,1)S(1)} all-gather(bf16[1,4,128]{2,1,0:T(4,128)(2,1)S(1)} %fusion.75), channel_id=2, replica_groups=mesh['sp_0'=8,'sp_1'=8,'fs'=4,'tp'=2] {'sp_1'}, dimensions={0}, use_global_device_ids=true | all-gather | bytes 9216 | tf_op jit(solution)/shard_map/all_gather | solution.py:52
  189.6 14.1 %all_gather.39 = bf16[8,4,128]{2,1,0:T(4,128)(2,1)S(1)} all-gather(bf16[1,4,128]{2,1,0:T(4,128)(2,1)S(1)} %fusion.65), channel_id=1, replica_groups=mesh['sp_0'=8,'sp_1'=8,'fs'=4,'tp'=2] {'sp_0'}, dimensions={0}, use_global_device_ids=true | all-gather | bytes 9216 | tf_op jit(solution)/shard_map/all_gather | solution.py:52
  203.8 5.7 %all-gather.14.cloned.1.call-done = bf16[32,128,128]{2,1,0:T(8,128)(2,1)} async-done(((bf16[4,128,128]{2,1,0:T(8,128)(2,1)}), bf16[32,128,128]{2,1,0:T(8,128)(2,1)}) %all-gather.14.cloned.1.call-update) | async-done | bytes 1048592 | tf_op jit(solution)/shard_map/all_gather | solution.py:52
  209.4 2.4 fusion.52
  211.9 2.7 collective-permute-start
  214.6 0.5 convolution_multiply_fusion
  215.2 0.3 fusion.62
  215.5 0.5 fusion.90
  216.0 0.5 convolution_bitcast_fusion
  216.5 0.1 copy.164
  216.7 0.1 fusion.47
  216.8 36.3 %all-gather.12.cloned.1.call-done = bf16[8,4,128,128]{3,2,1,0:T(8,128)(2,1)} async-done(((bf16[1,4,128,128]{3,2,1,0:T(8,128)(2,1)}), bf16[8,4,128,128]{3,2,1,0:T(8,128)(2,1)}) %all-gather.12.cloned.1.call-update) | async-done | bytes 1048592 | tf_op jit(solution)/shard_map/all_gather | solution.py:52
  253.1 2.9 %fusion.44 = f32[4,128,128]{2,1,0:T(8,128)S(1)} fusion(bf16[8,4,128,128]{3,2,1,0:T(8,128)(2,1)} %all-gather.12.cloned.1.call-done, f32[4,128]{1,0:T(4,128)S(1)} %get-tuple-element.90, f32[4,128]{1,0:T(4,128)S(1)} %get-tuple-element.104, f32[4,128]{1,0:T(4,128)S(1)} %get-tuple-element.103, f32[4,128]{1,0:T(4,128)S(1)} %get-tuple-element.102, ...), kind=kLoop, calls=%fused_computation.80 | loop fusion | flops 4194304 | bytes 2394128 | tf_op jit(solution)/shard_map/mul | solution.py:183
  256.1 0.8 multiply_reduce_fusion
  256.9 0.3 copy.178
  257.1 0.3 reshape.475
  257.4 0.1 rsqrt.21
  257.5 0.1 fusion.46
  257.7 3.7 %convolution_convert_fusion.1 = bf16[128,2048]{1,0:T(8,128)(2,1)S(1)} fusion(bf16[1024,2048]{0,1:T(8,128)(2,1)} %bitcast.378, bf16[128,512]{0,1:T(8,128)(2,1)S(1)} %fusion.46, bf16[128,512]{0,1:T(8,128)(2,1)S(1)} %fusion.47), kind=kOutput, calls=%fused_computation.4 | convolution fusion | flops 537657344 | bytes 4980736 | tf_op jit(solution)/shard_map/dot_general | solution.py:191
  261.4 9.1 %all_to_all.5 = bf16[2,64,2048]{2,1,0:T(8,128)(2,1)S(1)} all-to-all(bf16[2,64,2048]{2,1,0:T(8,128)(2,1)S(1)} %bitcast.380), channel_id=1, replica_groups=mesh['sp_0'=8,'sp_1'=8,'fs'=4,'tp'=2] {'tp'}, dimensions={0} | all-to-all | bytes 1048576 | tf_op jit(solution)/shard_map/all_to_all | solution.py:74
  270.5 0.8 reduce_sum.42
  (47 shorter events, 0.4 us)
Async XLA Ops:
  6.5 209.5 %copy-start = (bf16[2,256,256]{2,1,0:T(8,128)(2,1)S(1)}, bf16[2,256,256]{2,1,0:T(8,128)(2,1)}, u32[]{:S(2)}) copy-start(bf16[2,256,256]{2,1,0:T(8,128)(2,1)} %param.21) | copy-start | bytes 786436
  6.5 108.3 %all-gather.10.cloned.1.call-start = ((), (), s32[]{:S(2)}) async-start(), calls=%async_computation.1 | async-start | bytes 8519680 | tf_op jit(solution)/shard_map/all_gather | solution.py:113
  8.1 164.1 %all-gather.16.cloned.1.call-start = ((), (), s32[]{:S(2)}) async-start(), calls=%async_computation.4 | async-start | bytes 4718592 | tf_op jit(solution)/shard_map/all_gather | solution.py:23
  37.4 172.1 %all-gather.14.cloned.1.call-start = ((), (), s32[]{:S(2)}) async-start(), calls=%async_computation.3 | async-start | bytes 1179648 | tf_op jit(solution)/shard_map/all_gather | solution.py:52
  122.4 130.7 %all-gather.12.cloned.1.call-start = ((), (), s32[]{:S(2)}) async-start(), calls=%async_computation.2 | async-start | bytes 1179648 | tf_op jit(solution)/shard_map/all_gather | solution.py:52
  211.9 3.5 %collective-permute-start = (bf16[16,512]{1,0:T(8,128)(2,1)S(1)}, bf16[16,512]{1,0:T(8,128)(2,1)S(1)}, u32[]{:S(2)}, u32[]{:S(2)}) collective-permute-start(bf16[16,512]{1,0:T(8,128)(2,1)S(1)} %slice.306), channel_id=1, source_target_pairs={{0,8},{8,16},{16,24},{24,32},{32,40},{40,48},{48,56},{56,64},{64,7... | collective-permute-start | bytes 49160 | tf_op jit(solution)/shard_map/ppermute | solution.py:37
  216.0 0.7 copy-start.2
  216.0 37.1 %copy-start.1 = (bf16[32,128,128]{2,1,0:T(8,128)(2,1)S(1)}, bf16[32,128,128]{2,1,0:T(8,128)(2,1)}, u32[]{:S(2)}) copy-start(bf16[32,128,128]{2,1,0:T(8,128)(2,1)} %all-gather.14.cloned.1.call-done) | copy-start | bytes 3145732
  216.5 41.0 %copy-start.3 = (f32[512]{0:T(512)S(1)}, f32[512]{0:T(512)}, u32[]{:S(2)}) copy-start(f32[512]{0:T(512)} %param.25) | copy-start | bytes 6148
Sparse Core Ops, SparseCore 0:
  10.4 104.4 all-gather.9
  117.0 55.1 all-gather.15
  174.3 35.1 all-gather.13
  212.0 41.0 all-gather.11
where the time goes:
time: 279 us; the launch traced here: 278 us
  waiting for transfers between devices  159 us (57%)
  blocking collectives  69.3 us (25%)
  between operations  13.5 us (5%)
  other arithmetic  11.6 us (4%)
  matrix products  11.1 us (4%)
  local copies, waits for them, and re-layouts  10 us (4%)
  starting transfers between devices  2.81 us (1%)
    all_gather x1, waiting for transfers between devices, body(): lax.all_gather(stacked, SP, axis=0, tiled=True)  67.8 us
    all_gather x1, waiting for transfers between devices, all_blocks(): tiles = lax.all_gather(tiles, axes[k])  49.5 us
    all_gather x2, waiting for transfers between devices, carried_in(): lax.all_gather(part.astype(kind), axis)  42 us
    all_gather x1, blocking collectives, all_blocks(): tiles = lax.all_gather(tiles, axes[k])  27.3 us
    all_gather x2, blocking collectives, carried_in(): lax.all_gather(part.astype(kind), axis)  25.1 us
    all_to_all x1, blocking collectives, summed_on_arrival(): lax.all_to_all(tiles, axis, split_axis=0, concat_axis=0, tiled=True)  9.09 us
    all_gather x1, blocking collectives, body(): gathered = lax.all_gather(tokens, 'tp', axis=1, tiled=True)[0]  7.83 us
    transpose x1, local copies, waits for them, and re-layouts, all_blocks(): tiles = tiles.transpose(*back, *range(len(axes), tiles.ndim))  6.47 us
  transfers between devices with their start and end apart: 5, of which 4 were waited for; matrix products, arithmetic and copies ran while one was open for 7% of the time, Pallas kernels for 0%

commit v1 on v0

--- a/solution.py
+++ b/solution.py
@@ -110,7 +110,9 @@
     )
     out_local = jnp.concatenate([pooling_output_weight, recurrent_output_weight], axis=0)
     projected = jnp.dot(
-        normed, lax.all_gather(stacked, SP, axis=0, tiled=True), preferred_element_type=jnp.float32
+        normed,
+        jnp.concatenate(lax.all_to_all(jnp.stack([stacked] * lax.axis_size(SP)), SP, 0, 0), axis=0),
+        preferred_element_type=jnp.float32,
     )
     out_full = gathered_by_axis(out_local, SP, (0, 1), 1)
     rounded = lax.optimization_barrier(projected.astype(jnp.bfloat16))

time: 279 us -> 452 us (1.62)
  blocking collectives: 69.3 us -> 289 us
  waiting for transfers between devices: 159 us -> 89.9 us
  starting transfers between devices: 2.81 us -> 20.6 us
    all_gather x1, blocking collectives: 27.3 us -> 236 us  [all_blocks(): tiles = lax.all_gather(tiles, axes[k])]
    all_gather x1 -> x0, waiting for transfers between devices: 67.8 us -> none  [body(): lax.all_gather(stacked, SP, axis=0, tiled=True)]
    all_to_all x0 -> x1, starting transfers between devices: none -> 17.5 us  [body(): lax.all_to_all(jnp.stack([stacked] * lax.axis_size(SP)), SP, 0, 0)]
    all_gather x2, blocking collectives: 25.1 us -> 31.9 us  [carried_in(): lax.all_gather(part.astype(kind), axis)]
  transfers between devices with their start and end apart: 5 -> 5, of which waited for: 4 -> 3; matrix products, arithmetic and copies ran while one was open for 7% -> 5% of each run, Pallas kernels for 0% -> 0%
where the time goes in v1:
time: 452 us
  blocking collectives  289 us (64%)
  waiting for transfers between devices  89.9 us (20%)
  starting transfers between devices  20.6 us (5%)
  local copies, waits for them, and re-layouts  14.3 us (3%)
  between operations  13.6 us (3%)
  other arithmetic  12.3 us (3%)
  matrix products  11.8 us (3%)
    all_gather x1, blocking collectives, all_blocks(): tiles = lax.all_gather(tiles, axes[k])  236 us
    all_gather x1, waiting for transfers between devices, all_blocks(): tiles = lax.all_gather(tiles, axes[k])  49.9 us
    all_gather x2, waiting for transfers between devices, carried_in(): lax.all_gather(part.astype(kind), axis)  39.9 us
    all_gather x2, blocking collectives, carried_in(): lax.all_gather(part.astype(kind), axis)  31.9 us
    all_to_all x1, starting transfers between devices, body(): lax.all_to_all(jnp.stack([stacked] * lax.axis_size(SP)), SP, 0, 0)  17.5 us
    all_gather x1, blocking collectives, body(): gathered = lax.all_gather(tokens, 'tp', axis=1, tiled=True)[0]  12 us
    all_to_all x1, blocking collectives, summed_on_arrival(): lax.all_to_all(tiles, axis, split_axis=0, concat_axis=0, tiled=True)  9.08 us
  transfers between devices with their start and end apart: 5, of which 3 were waited for; matrix products, arithmetic and copies ran while one was open for 5% of the time, Pallas kernels for 0%

profile of v1, /device:TPU:1, one launch (start us, length us, event | category | flops | bytes accessed | tf_op | source)
XLA Modules:
  0.0 451.7 jit_solution(7033305355287346072)
XLA Ops:
  6.5 0.9 pad_maximum_fusion
  7.4 4.3 stack.2
  11.7 17.5 %all-to-all-start = ((bf16[64,32,2048]{2,1,0:T(8,128)(2,1)}), bf16[64,32,2048]{2,1,0:T(8,128)(2,1)}, u32[]{:S(2)}, u32[]{:S(2)}) async-start(bf16[64,32,2048]{2,1,0:T(8,128)(2,1)} %stack.2), calls=%async_computation | async-start | bytes 16777216 | tf_op jit(solution)/shard_map/all_to_all | solution.py:114
  29.3 236.2 %all-gather.2 = bf16[8192,32]{0,1:T(8,128)(2,1)S(1)} all-gather(bf16[1024,32]{0,1:T(8,128)(2,1)S(1)} %pad_maximum_fusion.1), channel_id=4, replica_groups=mesh['sp_0'=8,'sp_1'=8,'fs'=4,'tp'=2] {'sp_0'}, dimensions={0}, use_global_device_ids=true | all-gather | bytes 589824 | tf_op jit(solution)/shard_map/all_gather | solution.py:23
  265.5 1.1 copy.197
  266.7 0.1 copy.177
  266.9 0.6 compare_convert_fusion.6
  267.5 0.6 compare_convert_fusion.8
  268.0 12.0 %all_gather.33 = bf16[1,128,2048]{2,1,0:T(8,128)(2,1)S(1)} all-gather(bf16[1,64,2048]{2,1,0:T(8,128)(2,1)S(1)} %copy-done.3), channel_id=1, replica_groups=mesh['sp_0'=8,'sp_1'=8,'fs'=4,'tp'=2] {'tp'}, dimensions={1}, use_global_device_ids=true | all-gather | bytes 786432 | tf_op jit(solution)/shard_map/all_gather | solution.py:103
  280.0 0.2 fusion.2
  280.2 4.7 %convolution_convert_fusion = bf16[128,2048]{1,0:T(8,128)(2,1)S(1)} fusion(bf16[2048,2048]{1,0:T(8,128)(2,1)} %bitcast.1, bf16[1,128,2048]{2,1,0:T(8,128)(2,1)S(1)} %all_gather.33, f32[2048]{0:T(1024)S(1)} %copy-done.4, f32[128]{0:T(128)S(1)} %add_rsqrt_fusion.1), kind=kOutput, calls=%fused_computation.3 | convolution fusion | flops 1075052544 | bytes 9445888 | tf_op jit(solution)/shard_map/dot_general | solution.py:112
  284.9 0.2 negate_log-plus-one_fusion
  285.1 0.1 reshape.404
  285.2 0.1 reshape.403
  285.3 0.1 reshape.405
  285.4 0.7 fusion.89
  286.1 0.2 fusion.54
  286.4 0.2 exponential_multiply_fusion
  286.6 0.6 fusion.48
  287.2 0.5 while.13
  287.3 0.2 bitcast_add_fusion.2
  287.5 0.2 bitcast_add_fusion.2
  287.7 0.7 convert_element_type.535
  288.5 0.6 compare_convert_fusion.10
  289.1 0.6 compare_convert_fusion.12
  289.7 0.5 compare_convert_fusion.14
  290.3 49.9 %all-gather.13.cloned.1.call-done = bf16[64,1024,32]{1,0,2:T(8,128)(2,1)} async-done(((bf16[8,1024,32]{1,0,2:T(8,128)(2,1)}), bf16[64,1024,32]{1,0,2:T(8,128)(2,1)}) %all-gather.13.cloned.1.call-update) | async-done | bytes 4194320 | tf_op jit(solution)/shard_map/all_gather | solution.py:23
  340.2 6.4 %copy.176 = bf16[8,8,1024,32]{2,3,1,0:T(8,128)(2,1)} copy(bf16[8,8,1024,32]{2,0,1,3:T(8,128)(2,1)} %bitcast.376) | data formatting | bytes 8388608 | tf_op jit(solution)/shard_map/transpose | solution.py:26
  346.7 11.0 %all-gather.4 = bf16[8,4,128]{2,1,0:T(4,128)(2,1)S(1)} all-gather(bf16[1,4,128]{2,1,0:T(4,128)(2,1)S(1)} %fusion.75), channel_id=2, replica_groups=mesh['sp_0'=8,'sp_1'=8,'fs'=4,'tp'=2] {'sp_1'}, dimensions={0}, use_global_device_ids=true | all-gather | bytes 9216 | tf_op jit(solution)/shard_map/all_gather | solution.py:52
  357.7 20.9 %all_gather.35 = bf16[8,4,128]{2,1,0:T(4,128)(2,1)S(1)} all-gather(bf16[1,4,128]{2,1,0:T(4,128)(2,1)S(1)} %fusion.65), channel_id=1, replica_groups=mesh['sp_0'=8,'sp_1'=8,'fs'=4,'tp'=2] {'sp_0'}, dimensions={0}, use_global_device_ids=true | all-gather | bytes 9216 | tf_op jit(solution)/shard_map/all_gather | solution.py:52
  378.6 4.6 %all-gather.11.cloned.1.call-done = bf16[32,128,128]{2,1,0:T(8,128)(2,1)} async-done(((bf16[4,128,128]{2,1,0:T(8,128)(2,1)}), bf16[32,128,128]{2,1,0:T(8,128)(2,1)}) %all-gather.11.cloned.1.call-update) | async-done | bytes 1048592 | tf_op jit(solution)/shard_map/all_gather | solution.py:52
  383.2 2.4 fusion.52
  385.7 3.0 collective-permute-start
  388.7 0.5 convolution_multiply_fusion
  389.3 0.3 fusion.62
  389.6 0.5 fusion.90
  390.1 1.2 convolution_bitcast_fusion
  391.3 0.1 copy.164
  391.5 0.1 fusion.47
  391.6 35.3 %all-gather.9.cloned.1.call-done = bf16[8,4,128,128]{3,2,1,0:T(8,128)(2,1)} async-done(((bf16[1,4,128,128]{3,2,1,0:T(8,128)(2,1)}), bf16[8,4,128,128]{3,2,1,0:T(8,128)(2,1)}) %all-gather.9.cloned.1.call-update) | async-done | bytes 1048592 | tf_op jit(solution)/shard_map/all_gather | solution.py:52
  426.9 2.9 fusion.44
  429.9 0.8 multiply_reduce_fusion
  430.7 0.3 copy.178
  430.9 0.3 reshape.494
  431.3 0.1 fusion.46
  431.5 3.7 convolution_convert_fusion.1
  435.2 9.1 %all_to_all.10 = bf16[2,64,2048]{2,1,0:T(8,128)(2,1)S(1)} all-to-all(bf16[2,64,2048]{2,1,0:T(8,128)(2,1)S(1)} %bitcast.377), channel_id=1, replica_groups=mesh['sp_0'=8,'sp_1'=8,'fs'=4,'tp'=2] {'tp'}, dimensions={0} | all-to-all | bytes 1048576 | tf_op jit(solution)/shard_map/all_to_all | solution.py:74
  444.3 0.8 reduce_sum.42
  (61 shorter events, 0.7 us)
Async XLA Ops:
  6.5 383.6 %copy-start = (bf16[2,256,256]{2,1,0:T(8,128)(2,1)S(1)}, bf16[2,256,256]{2,1,0:T(8,128)(2,1)}, u32[]{:S(2)}) copy-start(bf16[2,256,256]{2,1,0:T(8,128)(2,1)} %param.21) | copy-start | bytes 786436
  11.7 17.6 %copy-start.5 = (bf16[512,32]{0,1:T(8,128)(2,1)S(1)}, bf16[512,32]{0,1:T(8,128)(2,1)}, u32[]{:S(2)}) copy-start(bf16[512,32]{0,1:T(8,128)(2,1)} %param.27) | copy-start | bytes 98308
  11.7 17.6 %copy-start.6 = (bf16[512,32]{0,1:T(8,128)(2,1)S(1)}, bf16[512,32]{0,1:T(8,128)(2,1)}, u32[]{:S(2)}) copy-start(bf16[512,32]{0,1:T(8,128)(2,1)} %param.26) | copy-start | bytes 98308
  11.7 255.0 %copy-start.9 = (f32[1,128,4]{1,2,0:T(4,128)S(1)}, f32[1,128,4]{1,2,0:T(4,128)}, u32[]{:S(2)}) copy-start(f32[1,128,4]{1,2,0:T(4,128)} %param.24) | copy-start | bytes 6148
  11.7 256.3 %copy-start.3 = (bf16[1,64,2048]{2,1,0:T(8,128)(2,1)S(1)}, bf16[1,64,2048]{2,1,0:T(8,128)(2,1)}, u32[]{:S(2)}) copy-start(bf16[1,64,2048]{2,1,0:T(8,128)(2,1)} %param.15) | copy-start | bytes 786436
  11.7 268.5 %copy-start.10 = (f32[512]{0:T(512)S(1)}, f32[512]{0:T(512)}, u32[]{:S(2)}) copy-start(f32[512]{0:T(512)} %param.23) | copy-start | bytes 6148
  11.7 268.5 %copy-start.4 = (f32[2048]{0:T(1024)S(1)}, f32[2048]{0:T(1024)}, u32[]{:S(2)}) copy-start(f32[2048]{0:T(1024)} %param.16) | copy-start | bytes 24580
  11.7 268.5 %all-to-all-start = ((bf16[64,32,2048]{2,1,0:T(8,128)(2,1)}), bf16[64,32,2048]{2,1,0:T(8,128)(2,1)}, u32[]{:S(2)}, u32[]{:S(2)}) async-start(bf16[64,32,2048]{2,1,0:T(8,128)(2,1)} %stack.2), calls=%async_computation | async-start | bytes 16777216 | tf_op jit(solution)/shard_map/all_to_all | solution.py:114
  29.3 311.0 %all-gather.13.cloned.1.call-start = ((), (), s32[]{:S(2)}) async-start(), calls=%async_computation.4 | async-start | bytes 4718592 | tf_op jit(solution)/shard_map/all_gather | solution.py:23
  266.6 116.6 %all-gather.11.cloned.1.call-start = ((), (), s32[]{:S(2)}) async-start(), calls=%async_computation.3 | async-start | bytes 1179648 | tf_op jit(solution)/shard_map/all_gather | solution.py:52
  287.2 102.3 %copy-start.2 = (bf16[128,512]{1,0:T(8,128)(2,1)S(1)}, bf16[128,512]{1,0:T(8,128)(2,1)}, u32[]{:S(2)}) copy-start(bf16[128,512]{1,0:T(8,128)(2,1)} %get-tuple-element.65) | copy-start | bytes 393220
  288.4 138.5 %all-gather.9.cloned.1.call-start = ((), (), s32[]{:S(2)}) async-start(), calls=%async_computation.2 | async-start | bytes 1179648 | tf_op jit(solution)/shard_map/all_gather | solution.py:52
  383.2 8.2 %copy-start.7 = (f32[512]{0:T(512)S(1)}, f32[512]{0:T(512)}, u32[]{:S(2)}) copy-start(f32[512]{0:T(512)} %param.22) | copy-start | bytes 6148
  385.7 41.3 %copy-start.1 = (bf16[32,128,128]{2,1,0:T(8,128)(2,1)S(1)}, bf16[32,128,128]{2,1,0:T(8,128)(2,1)}, u32[]{:S(2)}) copy-start(bf16[32,128,128]{2,1,0:T(8,128)(2,1)} %all-gather.11.cloned.1.call-done) | copy-start | bytes 3145732
  385.7 3.8 collective-permute-start
  389.6 41.8 %copy-start.8 = (f32[512]{0:T(512)S(1)}, f32[512]{0:T(512)}, u32[]{:S(2)}) copy-start(f32[512]{0:T(512)} %param.25) | copy-start | bytes 6148
Sparse Core Ops, SparseCore 0:
  266.7 73.4 all-gather.12
  342.3 40.9 all-gather.10
  385.8 41.0 all-gather.8
